TPU v7x, 32 devices: a whole 2x2x4 slice. The times are simulated.
32 devices in a mesh: sp: 8 (over z, x), tp: 4 (over y, core).
Axes of the slice: x: 2, y: 2, z: 4, core: 2. Of those that a mesh axis runs over, the one named last changes fastest.
Arguments:
- residual: bfloat16 [4096, 2048], P(('sp', 'tp')), may hold values from -6 to 6
- query_small: bfloat16 [4096, 8, 128], P('sp', 'tp'), may hold values from -120 to 120
- key_small: bfloat16 [4096, 8, 128], P('sp', 'tp'), may hold values from -6 to 6
- value_small: bfloat16 [4096, 8, 128], P('sp', 'tp'), may hold values from -6 to 6
- query_large: bfloat16 [4096, 8, 256], P('sp', 'tp'), may hold values from -120 to 120
- key_large: bfloat16 [4096, 8, 256], P('sp', 'tp'), may hold values from -6 to 6
- value_large: bfloat16 [4096, 8, 128], P('sp', 'tp'), may hold values from -6 to 6
- lambda_small: float32 [8], P('tp'), may hold values from 0.3 to 0.8
- lambda_large: float32 [8], P('tp'), may hold values from 0.3 to 0.8
- head_gain: float32 [128], replicated, may hold values from 0.1 to 1.9
- output_small: bfloat16 [1024, 2048], P('tp'), may hold values from -0.125 to 0.125
- output_large: bfloat16 [1024, 2048], P('tp'), may hold values from -0.125 to 0.125
- norm_gain: float32 [2048], replicated, may hold values from 0.1 to 1.9
- gate_weight: bfloat16 [2048, 5632], P('sp', 'tp'), may hold values from -0.125 to 0.125
- up_weight: bfloat16 [2048, 5632], P('sp', 'tp'), may hold values from -0.125 to 0.125
- down_weight: bfloat16 [5632, 2048], P('tp', 'sp'), may hold values from -0.3125 to 0.3125
Outputs:
- block_output: bfloat16 [4096, 2048], P(('sp', 'tp'))
All inputs are finite; a program needn't handle non-finite values.
Results may differ from a plain program's by a relative error of at most 0.015.
Values may be sent and summed in bfloat16 or wider, within the bound.
No kernel may reach another device: no remote copies, remote signals or barrier semaphores. Data moves between devices by JAX's collectives and lax.ppermute only.
A program may use at most 128 MiB of HBM per device.

v0:
```python
import math
import jax
import jax.numpy as jnp
from jax import lax
from jax.sharding import PartitionSpec as P

residual_scale = 8.0**0.25
branch_scale = 0.8
norm_epsilon = 1e-05
masked_score = -1e30


def from_partner(value, axis, distance):
    mask = 2**distance
    pairs = [(source, source ^ mask) for source in range(lax.axis_size(axis))]
    return lax.ppermute(value, axis, pairs)


def layer_norm(values, gains):
    centered = values - jnp.mean(values, axis=-1, keepdims=True)
    variance = jnp.mean(centered * centered, axis=-1, keepdims=True)
    return centered * lax.rsqrt(variance + norm_epsilon) * gains


def empty_state(head_count, tokens, width):
    return (
        jnp.full((head_count, 2, tokens), masked_score, jnp.float32),
        jnp.zeros((head_count, 2, tokens), jnp.float32),
        jnp.zeros((head_count, 2, tokens, width), jnp.float32),
    )


def absorb_group(state, query_maps, key_block, value_block, key_index, query_index):
    running_max, totals, accumulated = state
    head_size = query_maps.shape[3]
    scores = jnp.einsum(
        "qhmd,khmd->hmqk", query_maps, key_block, preferred_element_type=jnp.float32
    ) * head_size ** (-0.5)
    visible = key_index[None, :] <= query_index[:, None]
    scores = jnp.where(visible, scores, masked_score)
    new_max = jnp.maximum(running_max, jnp.max(scores, axis=-1))
    fading = jnp.exp(running_max - new_max)
    weights = jnp.where(visible, jnp.exp(scores - new_max[..., None]), 0.0)
    totals = totals * fading + jnp.sum(weights, axis=-1)
    accumulated = accumulated * fading[..., None] + jnp.einsum(
        "hmqk,khe->hmqe",
        weights.astype(jnp.bfloat16),
        value_block,
        preferred_element_type=jnp.float32,
    )
    return (new_max, totals, accumulated)


def finish_group(state, lambdas, head_gain):
    running_max, totals, accumulated = state
    map_out = accumulated / totals[..., None]
    combined = map_out[:, 0] - lambdas[:, None, None] * map_out[:, 1]
    mean_square = jnp.mean(combined * combined, axis=-1, keepdims=True)
    normed = (combined * lax.rsqrt(mean_square + norm_epsilon) * head_gain * branch_scale).astype(
        jnp.bfloat16
    )
    head_count, tokens, width = normed.shape
    return jnp.transpose(normed, (1, 0, 2)).reshape(tokens, head_count * width)


def per_device(
    residual,
    query_small,
    key_small,
    value_small,
    query_large,
    key_large,
    value_large,
    lambda_small,
    lambda_large,
    head_gain,
    output_small,
    output_large,
    norm_gain,
    gate_weight,
    up_weight,
    down_weight,
):
    tokens = query_small.shape[0]
    half = tokens // 2
    own_rows = residual.shape[0]
    bit_count = lax.axis_size("sp").bit_length() - 1
    residual_all = lax.all_gather(residual, "tp", axis=0, tiled=True)
    heads_small = query_small.shape[1]
    heads_large = query_large.shape[1]
    value_width = value_small.shape[2]
    first_start = lax.axis_index("sp") * tokens
    later_small = query_small[half:]
    later_large = query_large[half:]
    for bit in range(bit_count):
        later_small, later_large = from_partner((later_small, later_large), "sp", bit)
    second_start = (lax.axis_size("sp") - 1 - lax.axis_index("sp")) * tokens + half
    halves = (
        (
            query_small[:half].reshape(half, heads_small, 2, -1),
            query_large[:half].reshape(half, heads_large, 2, -1),
            first_start + jnp.arange(half, dtype=jnp.int32),
        ),
        (
            later_small.reshape(half, heads_small, 2, -1),
            later_large.reshape(half, heads_large, 2, -1),
            second_start + jnp.arange(half, dtype=jnp.int32),
        ),
    )
    one_half = (
        empty_state(heads_small, half, value_width),
        empty_state(heads_large, half, value_width),
    )
    keys_first = lax.all_gather(key_small, "sp", axis=0, tiled=True)
    keys_second = lax.all_gather(key_large, "sp", axis=0, tiled=True)
    values_first = lax.all_gather(value_small, "sp", axis=0, tiled=True)
    values_second = lax.all_gather(value_large, "sp", axis=0, tiled=True)
    row_count = keys_first.shape[0]
    block_size = math.gcd(row_count, 512)
    number = row_count // block_size
    stacked = (
        keys_first.reshape(number, block_size, heads_small, 2, -1),
        keys_second.reshape(number, block_size, heads_large, 2, -1),
        values_first.reshape(number, block_size, heads_small, value_width),
        values_second.reshape(number, block_size, heads_large, value_width),
    )

    def step(carried, block_items):
        block_index, blocks = block_items
        key_index = block_index * block_size + jnp.arange(block_size, dtype=jnp.int32)
        updated = []
        for which in range(2):
            maps_small, maps_large, query_index = halves[which]

            def take(pair):
                return (
                    absorb_group(pair[0], maps_small, blocks[0], blocks[2], key_index, query_index),
                    absorb_group(pair[1], maps_large, blocks[1], blocks[3], key_index, query_index),
                )

            def leave(pair):
                return pair

            updated.append(
                lax.cond(key_index[0] <= query_index[half - 1], take, leave, carried[which])
            )
        return ((updated[0], updated[1]), None)

    result, unused = lax.scan(
        step, (one_half, one_half), (jnp.arange(number, dtype=jnp.int32), stacked)
    )
    first_states, second_states = result
    early_small = finish_group(first_states[0], lambda_small, head_gain)
    early_large = finish_group(first_states[1], lambda_large, head_gain)
    late_small = finish_group(second_states[0], lambda_small, head_gain)
    late_large = finish_group(second_states[1], lambda_large, head_gain)
    for bit in range(bit_count):
        late_small, late_large = from_partner((late_small, late_large), "sp", bit)
    attended_small = jnp.concatenate([early_small, late_small], axis=0)
    attended_large = jnp.concatenate([early_large, late_large], axis=0)
    mixed_sum = lax.psum(
        (
            jnp.dot(attended_small, output_small, preferred_element_type=jnp.float32)
            + jnp.dot(attended_large, output_large, preferred_element_type=jnp.float32)
        ).astype(jnp.bfloat16),
        "tp",
    ).astype(jnp.float32)
    whole_rows = layer_norm(
        residual_scale * residual_all.astype(jnp.float32) + mixed_sum, norm_gain
    ).astype(jnp.bfloat16)
    normed = lax.dynamic_slice_in_dim(whole_rows, lax.axis_index("tp") * own_rows, own_rows, 0)
    gate_rows = jnp.dot(
        whole_rows,
        lax.all_gather(gate_weight, "sp", axis=0, tiled=True),
        preferred_element_type=jnp.float32,
    )
    up_rows = jnp.dot(
        whole_rows,
        lax.all_gather(up_weight, "sp", axis=0, tiled=True),
        preferred_element_type=jnp.float32,
    )
    down_full = lax.all_gather(down_weight, "sp", axis=1, tiled=True)
    hidden = (jax.nn.silu(gate_rows) * up_rows).astype(jnp.bfloat16)
    down_sum = lax.psum_scatter(
        jnp.dot(hidden, down_full, preferred_element_type=jnp.float32).astype(jnp.bfloat16),
        "tp",
        scatter_dimension=0,
        tiled=True,
    ).astype(jnp.float32)
    return (residual_scale * normed.astype(jnp.float32) + 0.5 * down_sum).astype(jnp.bfloat16)


def solution(mesh):
    in_specs = (
        P(("sp", "tp"), None),
        P("sp", "tp", None),
        P("sp", "tp", None),
        P("sp", "tp", None),
        P("sp", "tp", None),
        P("sp", "tp", None),
        P("sp", "tp", None),
        P("tp"),
        P("tp"),
        P(),
        P("tp", None),
        P("tp", None),
        P(),
        P("sp", "tp"),
        P("sp", "tp"),
        P("tp", "sp"),
    )
    out_specs = P(("sp", "tp"), None)
    return jax.shard_map(
        per_device, mesh=mesh, in_specs=in_specs, out_specs=out_specs, check_vma=False
    )
```

profile of v0, /device:TPU:0, one launch (start us, length us, event | category | flops | bytes accessed | tf_op | source)
XLA Modules:
  0.0 791.7 jit_solution(11565010698791997182)
XLA Ops:
  12.2 3.0 collective-permute-start.3
  15.2 6.3 collective-permute-done.3
  25.1 3.5 collective-permute-done
  30.0 7.0 collective-permute-done.4
  43.6 29.2 %collective-permute-done.2 = bf16[256,2,128]{2,1,0:T(2,128)(2,1)S(1)} collective-permute-done((bf16[256,2,128]{2,1,0:T(2,128)(2,1)S(1)}, bf16[256,2,128]{2,1,0:T(2,128)(2,1)S(1)}, u32[]{:S(2)}, u32[]{:S(2)}) %collective-permute-start.2) | collective-permute-done | bytes 131104 | tf_op jit(solution)/shard_map/ppermute | solution.py:16
  73.8 9.7 %reshape.126 = bf16[8,512,2,2,64]{4,3,2,1,0:T(2,128)(2,1)} reshape(bf16[4096,2,128]{2,1,0:T(2,128)(2,1)} %all-gather.11.cloned.1.call-done) | data formatting | bytes 4194304 | tf_op jit(solution)/shard_map/reshape | solution.py:122
  83.5 10.6 %copy.56 = bf16[8,512,2,2,64]{1,4,3,2,0:T(8,128)(2,1)} copy(bf16[8,512,2,2,64]{4,3,2,1,0:T(2,128)(2,1)} %reshape.126) | data formatting | bytes 4194304 | tf_op jit(solution)/shard_map/while | solution.py:149
  94.1 54.6 %all-gather.15.cloned.1.call-done = bf16[4096,2,256]{2,1,0:T(2,128)(2,1)} async-done(((bf16[512,2,256]{2,1,0:T(2,128)(2,1)}), bf16[4096,2,256]{2,1,0:T(2,128)(2,1)}) %all-gather.15.cloned.1.call-update) | async-done | bytes 4194320 | tf_op jit(solution)/shard_map/all_gather | solution.py:115
  148.7 11.7 %reshape.127 = bf16[8,512,2,2,128]{4,3,2,1,0:T(2,128)(2,1)} reshape(bf16[4096,2,256]{2,1,0:T(2,128)(2,1)} %all-gather.15.cloned.1.call-done) | data formatting | bytes 8388608 | tf_op jit(solution)/shard_map/reshape | solution.py:123
  160.4 38.1 %all-gather.13.cloned.1.call-done = bf16[4096,2,128]{2,0,1:T(8,128)(2,1)} async-done(((bf16[512,2,128]{2,0,1:T(8,128)(2,1)}), bf16[4096,2,128]{2,0,1:T(8,128)(2,1)}) %all-gather.13.cloned.1.call-update) | async-done | bytes 2097168 | tf_op jit(solution)/shard_map/all_gather | solution.py:116
  198.5 49.7 %all-gather.17.cloned.1.call-done = bf16[4096,2,128]{2,0,1:T(8,128)(2,1)} async-done(((bf16[512,2,128]{2,0,1:T(8,128)(2,1)}), bf16[4096,2,128]{2,0,1:T(8,128)(2,1)}) %all-gather.17.cloned.1.call-update) | async-done | bytes 2097168 | tf_op jit(solution)/shard_map/all_gather | solution.py:117
  251.6 124.7 %while.32 = (s32[]{:T(128)}, f32[2,2,256]{2,1,0:T(2,128)S(1)}, f32[2,2,256]{2,1,0:T(2,128)S(1)}, f32[2,2,256,128]{3,2,1,0:T(8,128)}, f32[2,2,256]{2,1,0:T(2,128)...) while((s32[]{:T(128)}, f32[2,2,256]{2,1,0:T(2,128)S(1)}, ...), condition=%wide.region_13.14_spmd, body=%wide.region_0.13_spmd.sunk | while | flops 968106496 | bytes 58991568 | solution.py:149
  258.8 5.7 conditional.5
  266.5 5.8 conditional.4
  279.4 5.7 conditional.5
  294.2 5.7 conditional.5
  309.1 5.7 conditional.5
  323.9 5.7 conditional.5
  338.8 5.7 conditional.5
  353.6 5.7 conditional.5
  368.4 5.7 conditional.5
  386.6 2.9 collective-permute-done.9
  394.7 3.6 collective-permute-start.11
  398.3 2.8 collective-permute-start.8
  410.6 48.7 %all-reduce.2.cloned.1.call-done = bf16[512,2048]{1,0:T(8,128)(2,1)} async-done(((bf16[512,2048]{1,0:T(8,128)(2,1)}), bf16[512,2048]{1,0:T(8,128)(2,1)}) %all-reduce.2.cloned.1.call-update) | async-done | bytes 2097168 | tf_op jit(solution)/shard_map/psum | solution.py:161
  459.3 3.1 fusion.48
  465.9 88.0 %all-gather.19.cloned.1.call-done = bf16[2048,1408]{1,0:T(8,128)(2,1)} async-done(((bf16[256,1408]{1,0:T(8,128)(2,1)}), bf16[2048,1408]{1,0:T(8,128)(2,1)}) %all-gather.19.cloned.1.call-update) | async-done | bytes 5767184 | tf_op jit(solution)/shard_map/all_gather | solution.py:174
  553.9 8.2 %fusion.72 = f32[512,1408]{1,0:T(8,128)} fusion(bf16[512,2048]{1,0:T(8,128)(2,1)} %multiply_convert_fusion, bf16[2048,1408]{1,0:T(8,128)(2,1)} %all-gather.19.cloned.1.call-done), kind=kOutput, calls=%fused_computation.131 | convolution fusion | flops 2952790016 | bytes 10747904 | tf_op jit(solution)/shard_map/dot_general | solution.py:172
  562.1 84.5 %all-gather.21.cloned.1.call-done = bf16[2048,1408]{1,0:T(8,128)(2,1)} async-done(((bf16[256,1408]{1,0:T(8,128)(2,1)}), bf16[2048,1408]{1,0:T(8,128)(2,1)}) %all-gather.21.cloned.1.call-update) | async-done | bytes 5767184 | tf_op jit(solution)/shard_map/all_gather | solution.py:179
  646.6 93.4 %all-gather.23.cloned.1.call-done = bf16[1408,2048]{1,0:T(8,128)(2,1)} async-done(((bf16[1408,256]{1,0:T(8,128)(2,1)}), bf16[1408,2048]{1,0:T(8,128)(2,1)}) %all-gather.23.cloned.1.call-update) | async-done | bytes 5767184 | tf_op jit(solution)/shard_map/all_gather | solution.py:182
  740.0 13.3 %convolution_convert_fusion = bf16[512,2048]{1,0:T(8,128)(2,1)} fusion(bf16[1408,2048]{1,0:T(8,128)(2,1)} %all-gather.23.cloned.1.call-done, bf16[512,2048]{1,0:T(8,128)(2,1)S(1)} %copy-done.3, bf16[2048,1408]{1,0:T(8,128)(2,1)} %all-gather.21.cloned.1.call-done, f32[512,1408]{1,0:T(8,128)} %fusion.72), kind=kOutput, calls=%fused_computation.79 | convolution fusion | flops 5910953984 | bytes 18612224 | tf_op jit(solution)/shard_map/dot_general | solution.py:185
  753.3 29.5 %reduce-scatter.2.cloned.1.call-done = bf16[128,2048]{1,0:T(8,128)(2,1)} async-done(((bf16[512,2048]{1,0:T(8,128)(2,1)}), bf16[128,2048]{1,0:T(8,128)(2,1)}) %reduce-scatter.2.cloned.1.call-update) | async-done | bytes 524304 | tf_op jit(solution)/shard_map/reduce_scatter | solution.py:184
  (368 shorter events, 150.1 us)
Async XLA Ops:
  6.5 396.8 %copy-start = (bf16[256,2048]{1,0:T(8,128)(2,1)S(1)}, bf16[256,2048]{1,0:T(8,128)(2,1)}, u32[]{:S(2)}) copy-start(bf16[256,2048]{1,0:T(8,128)(2,1)} %param.33) | copy-start | bytes 3145732
  6.5 5.1 copy-start.17
  6.5 16.8 %copy-start.18 = (bf16[512,2,128]{2,1,0:T(2,128)(2,1)S(1)}, bf16[512,2,128]{2,1,0:T(2,128)(2,1)}, u32[]{:S(2)}) copy-start(bf16[512,2,128]{2,1,0:T(2,128)(2,1)} %param.23) | copy-start | bytes 786436
  6.5 67.3 %all-gather.11.cloned.1.call-start = ((), (), s32[]{:S(2)}) async-start(), calls=%async_computation.2 | async-start | bytes 2359296 | tf_op jit(solution)/shard_map/all_gather | solution.py:114
  7.3 141.4 %all-gather.15.cloned.1.call-start = ((), (), s32[]{:S(2)}) async-start(), calls=%async_computation.4 | async-start | bytes 4718592 | tf_op jit(solution)/shard_map/all_gather | solution.py:115
  8.0 190.5 %all-gather.13.cloned.1.call-start = ((), (), s32[]{:S(2)}) async-start(), calls=%async_computation.3 | async-start | bytes 2359296 | tf_op jit(solution)/shard_map/all_gather | solution.py:116
  9.8 238.4 %all-gather.17.cloned.1.call-start = ((), (), s32[]{:S(2)}) async-start(), calls=%async_computation.5 | async-start | bytes 2359296 | tf_op jit(solution)/shard_map/all_gather | solution.py:117
  11.5 399.0 %all-gather.9.cloned.1.call-start = ((), (), s32[]{:S(2)}) async-start(), calls=%async_computation.1 | async-start | bytes 2621440 | tf_op jit(solution)/shard_map/all_gather | solution.py:88
  12.2 9.3 %collective-permute-start.3 = (bf16[256,2,256]{0,2,1:T(8,128)(2,1)S(1)}, bf16[256,2,256]{0,2,1:T(8,128)(2,1)S(1)}, u32[]{:S(2)}, u32[]{:S(2)}) collective-permute-start(bf16[256,2,256]{0,2,1:T(8,128)(2,1)S(1)} %copy.82), channel_id=1, source_target_pairs={{0,4},{4,0},{8,12},{12,8},{16,20},{20,16},{24,28},{28,24},{1,5},{5... | collective-permute-start | bytes 786440 | tf_op jit(solution)/shard_map/ppermute | solution.py:16
  21.5 15.5 %collective-permute-start.4 = (bf16[256,2,256]{0,2,1:T(8,128)(2,1)S(1)}, bf16[256,2,256]{0,2,1:T(8,128)(2,1)S(1)}, u32[]{:S(2)}, u32[]{:S(2)}) collective-permute-start(bf16[256,2,256]{0,2,1:T(8,128)(2,1)S(1)} %collective-permute-done.3), channel_id=1, source_target_pairs={{0,8},{4,12},{8,0},{12,4},{16,24},{20,28},{24,16},{28,20},{1,9},{5... | collective-permute-start | bytes 786440 | tf_op jit(solution)/shard_map/ppermute | solution.py:16
  23.5 5.0 collective-permute-start
  28.5 12.9 %collective-permute-start.1 = (bf16[256,2,128]{2,1,0:T(2,128)(2,1)S(1)}, bf16[256,2,128]{2,1,0:T(2,128)(2,1)S(1)}, u32[]{:S(2)}, u32[]{:S(2)}) collective-permute-start(bf16[256,2,128]{2,1,0:T(2,128)(2,1)S(1)} %collective-permute-done), channel_id=1, source_target_pairs={{0,8},{4,12},{8,0},{12,4},{16,24},{20,28},{24,16},{28,20},{1,9},{5... | collective-permute-start | bytes 393224 | tf_op jit(solution)/shard_map/ppermute | solution.py:16
  37.0 35.9 %collective-permute-start.5 = (bf16[256,2,256]{0,2,1:T(8,128)(2,1)S(1)}, bf16[256,2,256]{0,2,1:T(8,128)(2,1)S(1)}, u32[]{:S(2)}, u32[]{:S(2)}) collective-permute-start(bf16[256,2,256]{0,2,1:T(8,128)(2,1)S(1)} %collective-permute-done.4), channel_id=1, source_target_pairs={{0,16},{4,20},{8,24},{12,28},{16,0},{20,4},{24,8},{28,12},{1,17},{... | collective-permute-start | bytes 786440 | tf_op jit(solution)/shard_map/ppermute | solution.py:16
  41.5 31.3 %collective-permute-start.2 = (bf16[256,2,128]{2,1,0:T(2,128)(2,1)S(1)}, bf16[256,2,128]{2,1,0:T(2,128)(2,1)S(1)}, u32[]{:S(2)}, u32[]{:S(2)}) collective-permute-start(bf16[256,2,128]{2,1,0:T(2,128)(2,1)S(1)} %collective-permute-done.1), channel_id=1, source_target_pairs={{0,16},{4,20},{8,24},{12,28},{16,0},{20,4},{24,8},{28,12},{1,17},{... | collective-permute-start | bytes 393224 | tf_op jit(solution)/shard_map/ppermute | solution.py:16
  43.0 416.3 %all-reduce.2.cloned.1.call-start = ((), (), s32[]{:S(2)}) async-start(), calls=%async_computation.6 | async-start | bytes 4194304 | tf_op jit(solution)/shard_map/psum | solution.py:161
  376.3 4.6 copy-start.11
  377.7 4.3 copy-start.6
  379.8 3.2 copy-start.21
  384.5 5.0 collective-permute-start.9
  385.1 6.5 collective-permute-start.6
  389.6 5.1 collective-permute-start.10
  391.6 6.7 collective-permute-start.7
  394.7 8.6 %collective-permute-start.11 = (bf16[256,256]{0,1:T(8,128)(2,1)S(1)}, bf16[256,256]{0,1:T(8,128)(2,1)S(1)}, u32[]{:S(2)}, u32[]{:S(2)}) collective-permute-start(bf16[256,256]{0,1:T(8,128)(2,1)S(1)} %collective-permute-done.10), channel_id=1, source_target_pairs={{0,16},{4,20},{8,24},{12,28},{16,0},{20,4},{24,8},{28,12},{1,17},{... | collective-permute-start | bytes 393224 | tf_op jit(solution)/shard_map/ppermute | solution.py:16
  398.3 7.9 collective-permute-start.8
  403.3 2.8 copy-start.16
  408.3 145.6 %all-gather.19.cloned.1.call-start = ((), (), s32[]{:S(2)}) async-start(), calls=%async_computation.7 | async-start | bytes 6488064 | tf_op jit(solution)/shard_map/all_gather | solution.py:174
  409.0 237.6 %all-gather.21.cloned.1.call-start = ((), (), s32[]{:S(2)}) async-start(), calls=%async_computation.8 | async-start | bytes 6488064 | tf_op jit(solution)/shard_map/all_gather | solution.py:179
  409.8 330.2 %all-gather.23.cloned.1.call-start = ((), (), s32[]{:S(2)}) async-start(), calls=%async_computation.9 | async-start | bytes 6488064 | tf_op jit(solution)/shard_map/all_gather | solution.py:182
  410.5 372.3 %reduce-scatter.2.cloned.1.call-start = ((), (), s32[]{:S(2)}) async-start(), calls=%async_computation.10 | async-start | bytes 2621440 | tf_op jit(solution)/shard_map/reduce_scatter | solution.py:184
  410.6 51.9 %copy-start.1 = (bf16[512,2048]{1,0:T(8,128)(2,1)S(1)}, bf16[512,2048]{1,0:T(8,128)(2,1)}, u32[]{:S(2)}) copy-start(bf16[512,2048]{1,0:T(8,128)(2,1)} %all-gather.9.cloned.1.call-done) | copy-start | bytes 6291460
  459.3 3.1 copy-start.2
  465.9 274.1 %copy-start.3 = (bf16[512,2048]{1,0:T(8,128)(2,1)S(1)}, bf16[512,2048]{1,0:T(8,128)(2,1)}, u32[]{:S(2)}) copy-start(bf16[512,2048]{1,0:T(8,128)(2,1)} %multiply_convert_fusion) | copy-start | bytes 6291460
  (41 other events, 45.9 us)
Sparse Core Ops, SparseCore 0:
  9.5 64.2 all-gather.10
  75.9 72.7 all-gather.14
  150.9 47.5 all-gather.12
  200.6 47.5 all-gather.16
  249.6 21.0 all-gather.8
  408.4 50.8 all-reduce.1
  461.5 92.3 all-gather.18
  556.1 90.4 all-gather.20
  648.7 91.2 all-gather.22
  753.4 29.3 reduce-scatter.1
where the time goes:
time: 794 us; the launch traced here: 792 us
  waiting for transfers between devices  548 us (69%)
  local copies, waits for them, and re-layouts  102 us (13%)
  matrix products  52.3 us (7%)
  loops' own time  26.4 us (3%)
  other arithmetic  25.5 us (3%)
  starting transfers between devices  23.7 us (3%)
  between operations  13.9 us (2%)
    all_gather x1, waiting for transfers between devices, per_device(): down_full = lax.all_gather(down_weight, 'sp', axis=1, tiled=True)  93.4 us
    all_gather x1, waiting for transfers between devices, per_device(): lax.all_gather(gate_weight, 'sp', axis=0, tiled=True)  88 us
    all_gather x1, waiting for transfers between devices, per_device(): lax.all_gather(up_weight, 'sp', axis=0, tiled=True)  84.5 us
    ppermute x12, waiting for transfers between devices, from_partner(): return lax.ppermute(value, axis, pairs)  57.4 us
    all_gather x1, waiting for transfers between devices, per_device(): keys_second = lax.all_gather(key_large, 'sp', axis=0, tiled=True)  54.6 us
    all_gather x1, waiting for transfers between devices, per_device(): values_second = lax.all_gather(value_large, 'sp', axis=0, tiled=True)  49.7 us
    psum x1, waiting for transfers between devices, per_device(): lax.psum((jnp.dot(attended_small, output_small, preferred_element_type=jn...  48.7 us
    all_gather x1, waiting for transfers between devices, per_device(): values_first = lax.all_gather(value_small, 'sp', axis=0, tiled=True)  38.1 us
  transfers between devices with their start and end apart: 22, of which 18 were waited for; matrix products, arithmetic and copies ran while one was open for 20% of the time, Pallas kernels for 0%

commit v1 on v0

--- a/solution.py
+++ b/solution.py
@@ -8,6 +8,13 @@
 branch_scale = 0.8
 norm_epsilon = 1e-05
 masked_score = -1e30
+
+
+def all_by_exchange(block, name, along):
+    peers = lax.axis_size(name)
+    shards = jnp.stack([block for _ in range(peers)])
+    shards = lax.all_to_all(shards, name, split_axis=0, concat_axis=0)
+    return jnp.concatenate(shards, axis=along)
 
 
 def from_partner(value, axis, distance):
@@ -175,9 +182,7 @@
         preferred_element_type=jnp.float32,
     )
     up_rows = jnp.dot(
-        whole_rows,
-        lax.all_gather(up_weight, "sp", axis=0, tiled=True),
-        preferred_element_type=jnp.float32,
+        whole_rows, all_by_exchange(up_weight, "sp", 0), preferred_element_type=jnp.float32
     )
     down_full = lax.all_gather(down_weight, "sp", axis=1, tiled=True)
     hidden = (jax.nn.silu(gate_rows) * up_rows).astype(jnp.bfloat16)

time: 794 us -> 758 us (0.955)
  waiting for transfers between devices: 548 us -> 504 us
    all_gather x1 -> x0, waiting for transfers between devices: 84.5 us -> none  [per_device(): lax.all_gather(up_weight, 'sp', axis=0, tiled=True)]
    all_gather x1, waiting for transfers between devices: 88 us -> 142 us  [per_device(): lax.all_gather(gate_weight, 'sp', axis=0, tiled=True)]
  transfers between devices with their start and end apart: 22 -> 22, of which waited for: 18 -> 17; matrix products, arithmetic and copies ran while one was open for 20% -> 21% of each run, Pallas kernels for 0% -> 0%
where the time goes in v1:
time: 758 us; the launch traced here: 755 us
  waiting for transfers between devices  504 us (66%)
  local copies, waits for them, and re-layouts  105 us (14%)
  matrix products  52.4 us (7%)
  loops' own time  27.8 us (4%)
  starting transfers between devices  27 us (4%)
  other arithmetic  25.5 us (3%)
  between operations  13.6 us (2%)
    all_gather x1, waiting for transfers between devices, per_device(): lax.all_gather(gate_weight, 'sp', axis=0, tiled=True)  142 us
    all_gather x1, waiting for transfers between devices, per_device(): down_full = lax.all_gather(down_weight, 'sp', axis=1, tiled=True)  85.8 us
    ppermute x12, waiting for transfers between devices, from_partner(): return lax.ppermute(value, axis, pairs)  58.9 us
    all_gather x1, waiting for transfers between devices, per_device(): keys_second = lax.all_gather(key_large, 'sp', axis=0, tiled=True)  54.6 us
    all_gather x1, waiting for transfers between devices, per_device(): values_second = lax.all_gather(value_large, 'sp', axis=0, tiled=True)  49.7 us
    psum x1, waiting for transfers between devices, per_device(): lax.psum((jnp.dot(attended_small, output_small, preferred_element_type=jn...  41.2 us
    all_gather x1, waiting for transfers between devices, per_device(): values_first = lax.all_gather(value_small, 'sp', axis=0, tiled=True)  38.1 us
    reduce_scatter x1, waiting for transfers between devices, per_device(): lax.psum_scatter(jnp.dot(hidden, down_full, preferred_element_type=jnp.fl...  29.5 us
  transfers between devices with their start and end apart: 22, of which 17 were waited for; matrix products, arithmetic and copies ran while one was open for 21% of the time, Pallas kernels for 0%

profile of v1, /device:TPU:0, one launch (start us, length us, event | category | flops | bytes accessed | tf_op | source)
XLA Modules:
  0.0 755.3 jit_solution(9991061391355939896)
XLA Ops:
  12.2 3.0 collective-permute-start.3
  15.2 6.3 collective-permute-done.3
  25.1 3.5 collective-permute-done
  30.0 7.0 collective-permute-done.4
  43.6 29.2 %collective-permute-done.2 = bf16[256,2,128]{2,1,0:T(2,128)(2,1)S(1)} collective-permute-done((bf16[256,2,128]{2,1,0:T(2,128)(2,1)S(1)}, bf16[256,2,128]{2,1,0:T(2,128)(2,1)S(1)}, u32[]{:S(2)}, u32[]{:S(2)}) %collective-permute-start.2) | collective-permute-done | bytes 131104 | tf_op jit(solution)/shard_map/ppermute | solution.py:23
  73.8 9.7 %reshape.132 = bf16[8,512,2,2,64]{4,3,2,1,0:T(2,128)(2,1)} reshape(bf16[4096,2,128]{2,1,0:T(2,128)(2,1)} %all-gather.10.cloned.1.call-done) | data formatting | bytes 4194304 | tf_op jit(solution)/shard_map/reshape | solution.py:129
  83.5 10.6 %copy.56 = bf16[8,512,2,2,64]{1,4,3,2,0:T(8,128)(2,1)} copy(bf16[8,512,2,2,64]{4,3,2,1,0:T(2,128)(2,1)} %reshape.132) | data formatting | bytes 4194304 | tf_op jit(solution)/shard_map/while | solution.py:156
  94.1 54.6 %all-gather.14.cloned.1.call-done = bf16[4096,2,256]{2,1,0:T(2,128)(2,1)} async-done(((bf16[512,2,256]{2,1,0:T(2,128)(2,1)}), bf16[4096,2,256]{2,1,0:T(2,128)(2,1)}) %all-gather.14.cloned.1.call-update) | async-done | bytes 4194320 | tf_op jit(solution)/shard_map/all_gather | solution.py:122
  148.7 11.7 %reshape.133 = bf16[8,512,2,2,128]{4,3,2,1,0:T(2,128)(2,1)} reshape(bf16[4096,2,256]{2,1,0:T(2,128)(2,1)} %all-gather.14.cloned.1.call-done) | data formatting | bytes 8388608 | tf_op jit(solution)/shard_map/reshape | solution.py:130
  160.4 38.1 %all-gather.12.cloned.1.call-done = bf16[4096,2,128]{2,0,1:T(8,128)(2,1)} async-done(((bf16[512,2,128]{2,0,1:T(8,128)(2,1)}), bf16[4096,2,128]{2,0,1:T(8,128)(2,1)}) %all-gather.12.cloned.1.call-update) | async-done | bytes 2097168 | tf_op jit(solution)/shard_map/all_gather | solution.py:123
  198.5 49.7 %all-gather.16.cloned.1.call-done = bf16[4096,2,128]{2,0,1:T(8,128)(2,1)} async-done(((bf16[512,2,128]{2,0,1:T(8,128)(2,1)}), bf16[4096,2,128]{2,0,1:T(8,128)(2,1)}) %all-gather.16.cloned.1.call-update) | async-done | bytes 2097168 | tf_op jit(solution)/shard_map/all_gather | solution.py:124
  251.6 126.6 %while.32 = (s32[]{:T(128)}, f32[2,2,256]{2,1,0:T(2,128)S(1)}, f32[2,2,256]{2,1,0:T(2,128)S(1)}, f32[2,2,256,128]{3,2,1,0:T(8,128)}, f32[2,2,256]{2,1,0:T(2,128)...) while((s32[]{:T(128)}, f32[2,2,256]{2,1,0:T(2,128)S(1)}, ...), condition=%wide.region_13.14_spmd, body=%wide.region_0.13_spmd.sunk | while | flops 968106496 | bytes 58991568 | solution.py:156
  259.0 5.8 conditional.5
  266.7 5.7 conditional.4
  279.8 5.8 conditional.5
  294.8 5.8 conditional.5
  309.9 5.8 conditional.5
  325.0 5.8 conditional.5
  340.1 5.8 conditional.5
  355.1 5.8 conditional.5
  370.2 5.8 conditional.5
  388.5 2.9 collective-permute-done.9
  394.8 2.9 collective-permute-done.10
  411.4 2.9 stack.2
  414.3 4.7 all-to-all-start
  419.8 41.2 %all-reduce.2.cloned.1.call-done = bf16[512,2048]{1,0:T(8,128)(2,1)} async-done(((bf16[512,2048]{1,0:T(8,128)(2,1)}), bf16[512,2048]{1,0:T(8,128)(2,1)}) %all-reduce.2.cloned.1.call-update) | async-done | bytes 2097168 | tf_op jit(solution)/shard_map/psum | solution.py:168
  461.0 3.1 fusion.48
  467.5 142.3 %all-gather.18.cloned.1.call-done = bf16[2048,1408]{1,0:T(8,128)(2,1)} async-done(((bf16[256,1408]{1,0:T(8,128)(2,1)}), bf16[2048,1408]{1,0:T(8,128)(2,1)}) %all-gather.18.cloned.1.call-update) | async-done | bytes 5767184 | tf_op jit(solution)/shard_map/all_gather | solution.py:181
  609.8 8.3 %fusion.72 = f32[512,1408]{1,0:T(8,128)} fusion(bf16[512,2048]{1,0:T(8,128)(2,1)} %multiply_convert_fusion, bf16[2048,1408]{1,0:T(8,128)(2,1)} %all-gather.18.cloned.1.call-done), kind=kOutput, calls=%fused_computation.131 | convolution fusion | flops 2952790016 | bytes 10747904 | tf_op jit(solution)/shard_map/dot_general | solution.py:179
  618.1 85.8 %all-gather.20.cloned.1.call-done = bf16[1408,2048]{1,0:T(8,128)(2,1)} async-done(((bf16[1408,256]{1,0:T(8,128)(2,1)}), bf16[1408,2048]{1,0:T(8,128)(2,1)}) %all-gather.20.cloned.1.call-update) | async-done | bytes 5767184 | tf_op jit(solution)/shard_map/all_gather | solution.py:187
  703.9 13.3 %convolution_convert_fusion = bf16[512,2048]{1,0:T(8,128)(2,1)} fusion(bf16[1408,2048]{1,0:T(8,128)(2,1)} %all-gather.20.cloned.1.call-done, bf16[512,2048]{1,0:T(8,128)(2,1)S(1)} %copy-done.3, bf16[2048,1408]{1,0:T(8,128)(2,1)} %bitcast.37, f32[512,1408]{1,0:T(8,128)} %fusion.72), kind=kOutput, calls=%fused_computation.79 | convolution fusion | flops 5910953984 | bytes 18612224 | tf_op jit(solution)/shard_map/dot_general | solution.py:190
  717.2 29.5 %reduce-scatter.2.cloned.1.call-done = bf16[128,2048]{1,0:T(8,128)(2,1)} async-done(((bf16[512,2048]{1,0:T(8,128)(2,1)}), bf16[128,2048]{1,0:T(8,128)(2,1)}) %reduce-scatter.2.cloned.1.call-update) | async-done | bytes 524304 | tf_op jit(solution)/shard_map/reduce_scatter | solution.py:189
  (370 shorter events, 153.8 us)
Async XLA Ops:
  6.5 398.8 %copy-start = (bf16[256,2048]{1,0:T(8,128)(2,1)S(1)}, bf16[256,2048]{1,0:T(8,128)(2,1)}, u32[]{:S(2)}) copy-start(bf16[256,2048]{1,0:T(8,128)(2,1)} %param.33) | copy-start | bytes 3145732
  6.5 5.1 copy-start.18
  6.5 16.8 %copy-start.19 = (bf16[512,2,128]{2,1,0:T(2,128)(2,1)S(1)}, bf16[512,2,128]{2,1,0:T(2,128)(2,1)}, u32[]{:S(2)}) copy-start(bf16[512,2,128]{2,1,0:T(2,128)(2,1)} %param.23) | copy-start | bytes 786436
  6.5 67.3 %all-gather.10.cloned.1.call-start = ((), (), s32[]{:S(2)}) async-start(), calls=%async_computation.3 | async-start | bytes 2359296 | tf_op jit(solution)/shard_map/all_gather | solution.py:121
  7.3 141.4 %all-gather.14.cloned.1.call-start = ((), (), s32[]{:S(2)}) async-start(), calls=%async_computation.5 | async-start | bytes 4718592 | tf_op jit(solution)/shard_map/all_gather | solution.py:122
  8.0 190.5 %all-gather.12.cloned.1.call-start = ((), (), s32[]{:S(2)}) async-start(), calls=%async_computation.4 | async-start | bytes 2359296 | tf_op jit(solution)/shard_map/all_gather | solution.py:123
  9.8 238.4 %all-gather.16.cloned.1.call-start = ((), (), s32[]{:S(2)}) async-start(), calls=%async_computation.6 | async-start | bytes 2359296 | tf_op jit(solution)/shard_map/all_gather | solution.py:124
  11.5 408.3 %all-gather.8.cloned.1.call-start = ((), (), s32[]{:S(2)}) async-start(), calls=%async_computation.2 | async-start | bytes 2621440 | tf_op jit(solution)/shard_map/all_gather | solution.py:95
  12.2 9.3 %collective-permute-start.3 = (bf16[256,2,256]{0,2,1:T(8,128)(2,1)S(1)}, bf16[256,2,256]{0,2,1:T(8,128)(2,1)S(1)}, u32[]{:S(2)}, u32[]{:S(2)}) collective-permute-start(bf16[256,2,256]{0,2,1:T(8,128)(2,1)S(1)} %copy.82), channel_id=1, source_target_pairs={{0,4},{4,0},{8,12},{12,8},{16,20},{20,16},{24,28},{28,24},{1,5},{5... | collective-permute-start | bytes 786440 | tf_op jit(solution)/shard_map/ppermute | solution.py:23
  21.5 15.5 %collective-permute-start.4 = (bf16[256,2,256]{0,2,1:T(8,128)(2,1)S(1)}, bf16[256,2,256]{0,2,1:T(8,128)(2,1)S(1)}, u32[]{:S(2)}, u32[]{:S(2)}) collective-permute-start(bf16[256,2,256]{0,2,1:T(8,128)(2,1)S(1)} %collective-permute-done.3), channel_id=1, source_target_pairs={{0,8},{4,12},{8,0},{12,4},{16,24},{20,28},{24,16},{28,20},{1,9},{5... | collective-permute-start | bytes 786440 | tf_op jit(solution)/shard_map/ppermute | solution.py:23
  23.5 5.0 collective-permute-start
  28.5 12.9 %collective-permute-start.1 = (bf16[256,2,128]{2,1,0:T(2,128)(2,1)S(1)}, bf16[256,2,128]{2,1,0:T(2,128)(2,1)S(1)}, u32[]{:S(2)}, u32[]{:S(2)}) collective-permute-start(bf16[256,2,128]{2,1,0:T(2,128)(2,1)S(1)} %collective-permute-done), channel_id=1, source_target_pairs={{0,8},{4,12},{8,0},{12,4},{16,24},{20,28},{24,16},{28,20},{1,9},{5... | collective-permute-start | bytes 393224 | tf_op jit(solution)/shard_map/ppermute | solution.py:23
  37.0 35.9 %collective-permute-start.5 = (bf16[256,2,256]{0,2,1:T(8,128)(2,1)S(1)}, bf16[256,2,256]{0,2,1:T(8,128)(2,1)S(1)}, u32[]{:S(2)}, u32[]{:S(2)}) collective-permute-start(bf16[256,2,256]{0,2,1:T(8,128)(2,1)S(1)} %collective-permute-done.4), channel_id=1, source_target_pairs={{0,16},{4,20},{8,24},{12,28},{16,0},{20,4},{24,8},{28,12},{1,17},{... | collective-permute-start | bytes 786440 | tf_op jit(solution)/shard_map/ppermute | solution.py:23
  41.5 31.3 %collective-permute-start.2 = (bf16[256,2,128]{2,1,0:T(2,128)(2,1)S(1)}, bf16[256,2,128]{2,1,0:T(2,128)(2,1)S(1)}, u32[]{:S(2)}, u32[]{:S(2)}) collective-permute-start(bf16[256,2,128]{2,1,0:T(2,128)(2,1)S(1)} %collective-permute-done.1), channel_id=1, source_target_pairs={{0,16},{4,20},{8,24},{12,28},{16,0},{20,4},{24,8},{28,12},{1,17},{... | collective-permute-start | bytes 393224 | tf_op jit(solution)/shard_map/ppermute | solution.py:23
  43.0 418.0 %all-reduce.2.cloned.1.call-start = ((), (), s32[]{:S(2)}) async-start(), calls=%async_computation.7 | async-start | bytes 4194304 | tf_op jit(solution)/shard_map/psum | solution.py:168
  378.2 4.6 copy-start.11
  379.5 4.3 copy-start.6
  381.6 3.2 copy-start.22
  386.4 5.0 collective-permute-start.9
  386.9 6.5 collective-permute-start.6
  391.4 6.2 collective-permute-start.10
  393.4 6.6 collective-permute-start.7
  397.6 7.7 %collective-permute-start.11 = (bf16[256,256]{0,1:T(8,128)(2,1)S(1)}, bf16[256,256]{0,1:T(8,128)(2,1)S(1)}, u32[]{:S(2)}, u32[]{:S(2)}) collective-permute-start(bf16[256,256]{0,1:T(8,128)(2,1)S(1)} %collective-permute-done.10), channel_id=1, source_target_pairs={{0,16},{4,20},{8,24},{12,28},{16,0},{20,4},{24,8},{28,12},{1,17},{... | collective-permute-start | bytes 393224 | tf_op jit(solution)/shard_map/ppermute | solution.py:23
  399.9 8.2 %collective-permute-start.8 = (bf16[256,256]{0,1:T(8,128)(2,1)S(1)}, bf16[256,256]{0,1:T(8,128)(2,1)S(1)}, u32[]{:S(2)}, u32[]{:S(2)}) collective-permute-start(bf16[256,256]{0,1:T(8,128)(2,1)S(1)} %collective-permute-done.7), channel_id=1, source_target_pairs={{0,16},{4,20},{8,24},{12,28},{16,0},{20,4},{24,8},{28,12},{1,17},{... | collective-permute-start | bytes 393224 | tf_op jit(solution)/shard_map/ppermute | solution.py:23
  405.4 2.8 copy-start.16
  410.3 199.5 %all-gather.18.cloned.1.call-start = ((), (), s32[]{:S(2)}) async-start(), calls=%async_computation.8 | async-start | bytes 6488064 | tf_op jit(solution)/shard_map/all_gather | solution.py:181
  414.3 203.8 %all-to-all-start = ((bf16[8,256,1408]{2,1,0:T(8,128)(2,1)}), bf16[8,256,1408]{2,1,0:T(8,128)(2,1)}, u32[]{:S(2)}, u32[]{:S(2)}) async-start(bf16[8,256,1408]{2,1,0:T(8,128)(2,1)} %stack.2), calls=%async_computation | async-start | bytes 11534336 | tf_op jit(solution)/shard_map/all_to_all | solution.py:16
  419.0 284.9 %all-gather.20.cloned.1.call-start = ((), (), s32[]{:S(2)}) async-start(), calls=%async_computation.9 | async-start | bytes 6488064 | tf_op jit(solution)/shard_map/all_gather | solution.py:187
  419.8 327.0 %reduce-scatter.2.cloned.1.call-start = ((), (), s32[]{:S(2)}) async-start(), calls=%async_computation.10 | async-start | bytes 2621440 | tf_op jit(solution)/shard_map/reduce_scatter | solution.py:189
  419.8 44.3 %copy-start.1 = (bf16[512,2048]{1,0:T(8,128)(2,1)S(1)}, bf16[512,2048]{1,0:T(8,128)(2,1)}, u32[]{:S(2)}) copy-start(bf16[512,2048]{1,0:T(8,128)(2,1)} %all-gather.8.cloned.1.call-done) | copy-start | bytes 6291460
  461.0 3.1 copy-start.2
  467.5 236.4 %copy-start.3 = (bf16[512,2048]{1,0:T(8,128)(2,1)S(1)}, bf16[512,2048]{1,0:T(8,128)(2,1)}, u32[]{:S(2)}) copy-start(bf16[512,2048]{1,0:T(8,128)(2,1)} %multiply_convert_fusion) | copy-start | bytes 6291460
  (42 other events, 47.2 us)
Sparse Core Ops, SparseCore 0:
  9.5 64.2 all-gather.9
  75.9 72.7 all-gather.13
  150.9 47.5 all-gather.11
  200.6 47.5 all-gather.15
  249.6 21.0 all-gather.7
  410.4 50.5 all-reduce.1
  463.2 146.5 all-gather.17
  611.8 92.0 all-gather.19
  717.3 29.3 reduce-scatter.1
